TPU v7x, 32 devices: a whole 2x2x4 slice. The times are simulated.
32 devices in a mesh: rep: 2 (over x), fs: 8 (over z, y), tp: 2 (over core).
Axes of the slice: x: 2, y: 2, z: 4, core: 2. Of those that a mesh axis runs over, the one named last changes fastest.
Arguments:
- tokens: bfloat16 [4096, 2048], P(('rep', 'fs', 'tp')), may hold values from -6 to 6
- mix_gain: float32 [2048], replicated, may hold values from 0.1 to 1.9
- conv_in_weight: bfloat16 [2048, 1024], P('fs', 'tp'), may hold values from -0.125 to 0.125
- gate_outer_weight: bfloat16 [2048, 1024], P('fs', 'tp'), may hold values from -0.125 to 0.125
- gate_inner_weight: bfloat16 [2048, 1024], P('fs', 'tp'), may hold values from -0.125 to 0.125
- conv_taps: float32 [3, 1024], P(None, 'tp'), may hold values from -3.5 to 3.5
- out_weight: bfloat16 [1024, 2048], P('tp', 'fs'), may hold values from -0.1875 to 0.1875
- ff_gain: float32 [2048], replicated, may hold values from 0.1 to 1.9
- up_weight: bfloat16 [2048, 8192], P('fs', 'tp'), may hold values from -0.125 to 0.125
- down_weight: bfloat16 [8192, 2048], P('tp', 'fs'), may hold values from -0.0625 to 0.0625
Outputs:
- layer_out: bfloat16 [4096, 2048], P(('rep', 'fs', 'tp'))
All inputs are finite; a program needn't handle non-finite values.
Results may differ from a plain program's by a relative error of at most 0.023.
Values may be sent and summed in bfloat16 or wider, within the bound.
A program may use at most 128 MiB of HBM per device.

v0:
```python
import jax
import jax.numpy as jnp
from jax import lax
from jax.sharding import PartitionSpec as P

eps = 1e-06


def rms_scale(values, gain):
    widened = values.astype(jnp.float32)
    inverse = lax.rsqrt(jnp.mean(widened * widened, axis=-1, keepdims=True) + eps)
    return (widened * inverse * gain).astype(jnp.bfloat16)


def on_device(
    tokens,
    mix_gain,
    conv_in_weight,
    gate_outer_weight,
    gate_inner_weight,
    conv_taps,
    out_weight,
    ff_gain,
    up_weight,
    down_weight,
):
    normed = rms_scale(tokens, mix_gain)
    gathered = lax.all_gather(normed, "tp", axis=0, tiled=True)
    seq_rows = gathered.shape[0]
    segment = (
        lax.all_gather(conv_in_weight, "fs", axis=0, tiled=True),
        lax.all_gather(gate_outer_weight, "fs", axis=0, tiled=True),
        lax.all_gather(gate_inner_weight, "fs", axis=0, tiled=True),
    )
    conv_input, gate_outer, gate_inner = tuple(
        (jnp.dot(gathered, weight, preferred_element_type=jnp.float32) for weight in segment)
    )
    conv_input = conv_input.astype(jnp.bfloat16)
    gate_outer = gate_outer.astype(jnp.bfloat16)
    gate_inner = gate_inner.astype(jnp.bfloat16)
    gated = gate_inner.astype(jnp.float32) * conv_input.astype(jnp.float32)
    padded = jnp.pad(gated, ((2, 0), (0, 0)))
    convolved = (
        conv_taps[0] * padded[0:seq_rows]
        + conv_taps[1] * padded[1 : seq_rows + 1]
        + conv_taps[2] * padded[2 : seq_rows + 2]
    )
    mixed = (gate_outer.astype(jnp.float32) * convolved).astype(jnp.bfloat16)
    out_full = lax.all_gather(out_weight, "fs", axis=1, tiled=True)
    lefts = mixed
    mix_total = lax.psum_scatter(
        jnp.dot(lefts, out_full, preferred_element_type=jnp.float32).astype(jnp.bfloat16),
        "tp",
        scatter_dimension=0,
        tiled=True,
    ).astype(jnp.float32)
    resid = (tokens.astype(jnp.float32) + mix_total).astype(jnp.bfloat16)
    normed_ff = rms_scale(resid, ff_gain)
    ff_gathered = lax.all_gather(normed_ff, "tp", axis=0, tiled=True)
    up_full = lax.all_gather(up_weight, "fs", axis=0, tiled=True)
    preact = jnp.dot(ff_gathered, up_full, preferred_element_type=jnp.float32)
    hidden = jnp.square(jax.nn.relu(preact)).astype(jnp.bfloat16)
    down_full = lax.all_gather(down_weight, "fs", axis=1, tiled=True)
    lefts = hidden
    ff_total = lax.psum_scatter(
        jnp.dot(lefts, down_full, preferred_element_type=jnp.float32).astype(jnp.bfloat16),
        "tp",
        scatter_dimension=0,
        tiled=True,
    ).astype(jnp.float32)
    return (resid.astype(jnp.float32) + ff_total).astype(jnp.bfloat16)


def solution(mesh):
    in_specs = (
        P(("rep", "fs", "tp"), None),
        P(),
        P("fs", "tp"),
        P("fs", "tp"),
        P("fs", "tp"),
        P(None, "tp"),
        P("tp", "fs"),
        P(),
        P("fs", "tp"),
        P("tp", "fs"),
    )
    out_specs = P(("rep", "fs", "tp"), None)
    return jax.shard_map(
        on_device, mesh=mesh, in_specs=in_specs, out_specs=out_specs, check_vma=False
    )
```

profile of v0, /device:TPU:0, one launch (start us, length us, event | category | flops | bytes accessed | tf_op | source)
XLA Modules:
  0.0 740.0 jit_solution(13610082769893983982)
XLA Ops:
  6.5 1.2 fusion.8
  7.8 2.0 fusion.10
  9.9 0.7 all-gather.15.cloned.1.call-update
  10.6 0.7 all-gather.13.cloned.1.call-update
  12.0 0.5 all-gather.17.cloned.1.call-update
  12.6 9.2 %all-gather.9.cloned.1.call-done = bf16[256,2048]{1,0:T(8,128)(2,1)} async-done(((bf16[128,2048]{1,0:T(8,128)(2,1)}), bf16[256,2048]{1,0:T(8,128)(2,1)}) %all-gather.9.cloned.1.call-update) | async-done | bytes 1048592 | tf_op jit(solution)/shard_map/all_gather | solution.py:28
  21.7 52.4 %all-gather.15.cloned.1.call-done = bf16[2048,512]{1,0:T(8,128)(2,1)} async-done(((bf16[256,512]{1,0:T(8,128)(2,1)}), bf16[2048,512]{1,0:T(8,128)(2,1)}) %all-gather.15.cloned.1.call-update) | async-done | bytes 2097168 | tf_op jit(solution)/shard_map/all_gather | solution.py:31
  74.2 2.6 fusion.7
  76.8 47.2 %all-gather.13.cloned.1.call-done = bf16[2048,512]{1,0:T(8,128)(2,1)} async-done(((bf16[256,512]{1,0:T(8,128)(2,1)}), bf16[2048,512]{1,0:T(8,128)(2,1)}) %all-gather.13.cloned.1.call-update) | async-done | bytes 2097168 | tf_op jit(solution)/shard_map/all_gather | solution.py:33
  124.0 2.3 fusion.6
  126.3 47.3 %all-gather.11.cloned.1.call-done = bf16[2048,512]{1,0:T(8,128)(2,1)} async-done(((bf16[256,512]{1,0:T(8,128)(2,1)}), bf16[2048,512]{1,0:T(8,128)(2,1)}) %all-gather.11.cloned.1.call-update) | async-done | bytes 2097168 | tf_op jit(solution)/shard_map/all_gather | solution.py:32
  173.6 50.8 %all-gather.17.cloned.1.call-done = bf16[512,2048]{1,0:T(8,128)(2,1)} async-done(((bf16[512,256]{1,0:T(8,128)(2,1)}), bf16[512,2048]{1,0:T(8,128)(2,1)}) %all-gather.17.cloned.1.call-update) | async-done | bytes 2097168 | tf_op jit(solution)/shard_map/all_gather | solution.py:49
  224.4 4.7 convolution_convert_fusion.1
  229.2 6.7 reduce-scatter.3.cloned.1.call-done
  235.9 1.3 fusion.12
  237.2 2.0 fusion.14
  239.3 0.7 all-gather.21.cloned.1.call-update
  240.0 0.7 all-gather.23.cloned.1.call-update
  240.8 8.9 %all-gather.19.cloned.1.call-done = bf16[256,2048]{1,0:T(8,128)(2,1)} async-done(((bf16[128,2048]{1,0:T(8,128)(2,1)}), bf16[256,2048]{1,0:T(8,128)(2,1)}) %all-gather.19.cloned.1.call-update) | async-done | bytes 1048592 | tf_op jit(solution)/shard_map/all_gather | solution.py:59
  249.6 230.6 %all-gather.21.cloned.1.call-done = bf16[2048,4096]{1,0:T(8,128)(2,1)} async-done(((bf16[256,4096]{1,0:T(8,128)(2,1)}), bf16[2048,4096]{1,0:T(8,128)(2,1)}) %all-gather.21.cloned.1.call-update) | async-done | bytes 16777232 | tf_op jit(solution)/shard_map/all_gather | solution.py:60
  480.2 227.6 %all-gather.23.cloned.1.call-done = bf16[4096,2048]{1,0:T(8,128)(2,1)} async-done(((bf16[4096,256]{1,0:T(8,128)(2,1)}), bf16[4096,2048]{1,0:T(8,128)(2,1)}) %all-gather.23.cloned.1.call-update) | async-done | bytes 16777232 | tf_op jit(solution)/shard_map/all_gather | solution.py:63
  707.8 16.5 %convolution_convert_fusion = bf16[256,2048]{1,0:T(8,128)(2,1)} fusion(bf16[4096,2048]{1,0:T(8,128)(2,1)} %all-gather.23.cloned.1.call-done, bf16[256,2048]{1,0:T(8,128)(2,1)} %all-gather.19.cloned.1.call-done, bf16[2048,4096]{1,0:T(8,128)(2,1)} %all-gather.21.cloned.1.call-done), kind=kOutput, calls=%fused_computation.3 | convolution fusion | flops 8593604608 | bytes 35651584 | tf_op jit(solution)/shard_map/dot_general | solution.py:66
  724.4 6.7 reduce-scatter.5.cloned.1.call-done
  731.1 2.1 fusion.15
  (28 shorter events, 1.0 us)
Async XLA Ops:
  6.5 6.0 copy-start.4
  6.5 15.2 %all-gather.9.cloned.1.call-start = ((), (), s32[]{:S(2)}) async-start(), calls=%async_computation.2 | async-start | bytes 1572864 | tf_op jit(solution)/shard_map/all_gather | solution.py:28
  9.8 64.3 %all-gather.15.cloned.1.call-start = ((), (), s32[]{:S(2)}) async-start(), calls=%async_computation.5 | async-start | bytes 2359296 | tf_op jit(solution)/shard_map/all_gather | solution.py:31
  10.6 113.4 %all-gather.13.cloned.1.call-start = ((), (), s32[]{:S(2)}) async-start(), calls=%async_computation.4 | async-start | bytes 2359296 | tf_op jit(solution)/shard_map/all_gather | solution.py:33
  11.3 162.3 %all-gather.11.cloned.1.call-start = ((), (), s32[]{:S(2)}) async-start(), calls=%async_computation.3 | async-start | bytes 2359296 | tf_op jit(solution)/shard_map/all_gather | solution.py:32
  11.9 212.5 %all-gather.17.cloned.1.call-start = ((), (), s32[]{:S(2)}) async-start(), calls=%async_computation.6 | async-start | bytes 2359296 | tf_op jit(solution)/shard_map/all_gather | solution.py:49
  12.5 223.4 %reduce-scatter.3.cloned.1.call-start = ((), (), s32[]{:S(2)}) async-start(), calls=%async_computation.7 | async-start | bytes 1572864 | tf_op jit(solution)/shard_map/reduce_scatter | solution.py:51
  21.7 102.2 %copy-start.2 = (bf16[256,2048]{1,0:T(8,128)(2,1)S(1)}, bf16[256,2048]{1,0:T(8,128)(2,1)}, u32[]{:S(2)}) copy-start(bf16[256,2048]{1,0:T(8,128)(2,1)} %all-gather.9.cloned.1.call-done) | copy-start | bytes 3145732
  224.4 11.5 %copy-start = (bf16[128,2048]{1,0:T(8,128)(2,1)S(1)}, bf16[128,2048]{1,0:T(8,128)(2,1)}, u32[]{:S(2)}) copy-start(bf16[128,2048]{1,0:T(8,128)(2,1)} %param.10) | copy-start | bytes 1572868
  229.1 8.1 %copy-start.3 = (f32[2048]{0:T(1024)S(1)}, f32[2048]{0:T(1024)}, u32[]{:S(2)}) copy-start(f32[2048]{0:T(1024)} %param.17) | copy-start | bytes 24580
  229.1 20.5 %all-gather.19.cloned.1.call-start = ((), (), s32[]{:S(2)}) async-start(), calls=%async_computation.8 | async-start | bytes 1572864 | tf_op jit(solution)/shard_map/all_gather | solution.py:59
  239.2 241.0 %all-gather.21.cloned.1.call-start = ((), (), s32[]{:S(2)}) async-start(), calls=%async_computation.9 | async-start | bytes 18874368 | tf_op jit(solution)/shard_map/all_gather | solution.py:60
  240.0 467.8 %all-gather.23.cloned.1.call-start = ((), (), s32[]{:S(2)}) async-start(), calls=%async_computation.10 | async-start | bytes 18874368 | tf_op jit(solution)/shard_map/all_gather | solution.py:63
  240.7 490.4 %copy-start.1 = (bf16[128,2048]{1,0:T(8,128)(2,1)S(1)}, bf16[128,2048]{1,0:T(8,128)(2,1)}, u32[]{:S(2)}) copy-start(bf16[128,2048]{1,0:T(8,128)(2,1)} %reduce-scatter.3.cloned.1.call-done) | copy-start | bytes 1572868
  240.7 490.4 %reduce-scatter.5.cloned.1.call-start = ((), (), s32[]{:S(2)}) async-start(), calls=%async_computation.11 | async-start | bytes 1572864 | tf_op jit(solution)/shard_map/reduce_scatter | solution.py:65
Sparse Core Ops, SparseCore 0:
  10.0 11.7 all-gather.8
  23.9 50.2 all-gather.14
  76.3 47.6 all-gather.12
  125.9 47.6 all-gather.10
  175.5 48.8 all-gather.16
  229.2 6.5 reduce-scatter.2
  239.3 10.2 all-gather.18
  251.7 228.4 all-gather.20
  482.3 225.4 all-gather.22
  724.5 6.5 reduce-scatter.4
where the time goes:
time: 740 us
  waiting for transfers between devices  691 us (93%)
  matrix products  26.2 us (4%)
  between operations  13.6 us (2%)
  other arithmetic  8.69 us (1%)
    all_gather x1, waiting for transfers between devices, on_device(): up_full = lax.all_gather(up_weight, 'fs', axis=0, tiled=True)  231 us
    all_gather x1, waiting for transfers between devices, on_device(): down_full = lax.all_gather(down_weight, 'fs', axis=1, tiled=True)  228 us
    all_gather x1, waiting for transfers between devices, on_device(): lax.all_gather(conv_in_weight, 'fs', axis=0, tiled=True)  52.4 us
    all_gather x1, waiting for transfers between devices, on_device(): out_full = lax.all_gather(out_weight, 'fs', axis=1, tiled=True)  50.8 us
    all_gather x1, waiting for transfers between devices, on_device(): lax.all_gather(gate_outer_weight, 'fs', axis=0, tiled=True)  47.3 us
    all_gather x1, waiting for transfers between devices, on_device(): lax.all_gather(gate_inner_weight, 'fs', axis=0, tiled=True)  47.2 us
    dot_general x1, matrix products, on_device(): jnp.dot(lefts, down_full, preferred_element_type=jnp.float32)  16.5 us
  transfers between devices with their start and end apart: 10, of which 10 were waited for; matrix products, arithmetic and copies ran while one was open for 1% of the time, Pallas kernels for 0%

commit v1 on v0

--- a/solution.py
+++ b/solution.py
@@ -4,6 +4,10 @@
 from jax.sharding import PartitionSpec as P
 
 eps = 1e-06
+
+
+def _number_modes(sample):
+    return jnp.concatenate(jax.lax.all_gather(sample, "fs"), axis=1)
 
 
 def rms_scale(values, gain):
@@ -46,7 +50,7 @@
         + conv_taps[2] * padded[2 : seq_rows + 2]
     )
     mixed = (gate_outer.astype(jnp.float32) * convolved).astype(jnp.bfloat16)
-    out_full = lax.all_gather(out_weight, "fs", axis=1, tiled=True)
+    out_full = _number_modes(out_weight)
     lefts = mixed
     mix_total = lax.psum_scatter(
         jnp.dot(lefts, out_full, preferred_element_type=jnp.float32).astype(jnp.bfloat16),

time: 740 us -> 738 us (level)
  transfers between devices with their start and end apart: 10 -> 10, of which waited for: 10 -> 10; matrix products, arithmetic and copies ran while one was open for 1% -> 2% of each run, Pallas kernels for 0% -> 0%
where the time goes in v1:
time: 738 us
  waiting for transfers between devices  686 us (93%)
  matrix products  26.1 us (4%)
  between operations  13.6 us (2%)
  other arithmetic  8.69 us (1%)
    all_gather x1, waiting for transfers between devices, on_device(): up_full = lax.all_gather(up_weight, 'fs', axis=0, tiled=True)  231 us
    all_gather x1, waiting for transfers between devices, on_device(): down_full = lax.all_gather(down_weight, 'fs', axis=1, tiled=True)  228 us
    all_gather x1, waiting for transfers between devices, on_device(): lax.all_gather(conv_in_weight, 'fs', axis=0, tiled=True)  52.4 us
    all_gather x1, waiting for transfers between devices, _number_modes(): return jnp.concatenate(jax.lax.all_gather(sample, 'fs'), axis=1)  48.7 us
    all_gather x1, waiting for transfers between devices, on_device(): lax.all_gather(gate_inner_weight, 'fs', axis=0, tiled=True)  47 us
    all_gather x1, waiting for transfers between devices, on_device(): lax.all_gather(gate_outer_weight, 'fs', axis=0, tiled=True)  47 us
    dot_general x1, matrix products, on_device(): jnp.dot(lefts, down_full, preferred_element_type=jnp.float32)  16.5 us
  transfers between devices with their start and end apart: 10, of which 10 were waited for; matrix products, arithmetic and copies ran while one was open for 2% of the time, Pallas kernels for 0%

profile of v1, /device:TPU:0, one launch (start us, length us, event | category | flops | bytes accessed | tf_op | source)
XLA Modules:
  0.0 737.7 jit_solution(13663034521417805884)
XLA Ops:
  6.5 0.7 all-gather.24.cloned.1.call-update
  7.3 1.2 fusion.8
  8.5 2.0 fusion.10
  10.6 0.7 all-gather.16.cloned.1.call-update
  12.6 48.7 %all-gather.24.cloned.1.call-done = bf16[4096,256]{1,0:T(8,128)(2,1)} async-done(((bf16[512,256]{1,0:T(8,128)(2,1)}), bf16[4096,256]{1,0:T(8,128)(2,1)}) %all-gather.24.cloned.1.call-update) | async-done | bytes 2097168 | tf_op jit(solution)/shard_map/all_gather | solution.py:10
  61.3 2.9 copy.11
  64.2 6.3 all-gather.10.cloned.1.call-done
  70.4 52.4 %all-gather.16.cloned.1.call-done = bf16[2048,512]{1,0:T(8,128)(2,1)} async-done(((bf16[256,512]{1,0:T(8,128)(2,1)}), bf16[2048,512]{1,0:T(8,128)(2,1)}) %all-gather.16.cloned.1.call-update) | async-done | bytes 2097168 | tf_op jit(solution)/shard_map/all_gather | solution.py:35
  122.9 2.6 fusion.7
  125.5 47.0 %all-gather.14.cloned.1.call-done = bf16[2048,512]{1,0:T(8,128)(2,1)} async-done(((bf16[256,512]{1,0:T(8,128)(2,1)}), bf16[2048,512]{1,0:T(8,128)(2,1)}) %all-gather.14.cloned.1.call-update) | async-done | bytes 2097168 | tf_op jit(solution)/shard_map/all_gather | solution.py:37
  172.5 2.6 fusion.6
  175.1 47.0 %all-gather.12.cloned.1.call-done = bf16[2048,512]{1,0:T(8,128)(2,1)} async-done(((bf16[256,512]{1,0:T(8,128)(2,1)}), bf16[2048,512]{1,0:T(8,128)(2,1)}) %all-gather.12.cloned.1.call-update) | async-done | bytes 2097168 | tf_op jit(solution)/shard_map/all_gather | solution.py:36
  222.1 4.3 convolution_convert_fusion.1
  226.5 7.0 reduce-scatter.3.cloned.1.call-done
  233.5 1.3 fusion.12
  234.9 2.0 fusion.14
  237.0 0.7 all-gather.20.cloned.1.call-update
  237.7 0.7 all-gather.22.cloned.1.call-update
  238.5 8.9 %all-gather.18.cloned.1.call-done = bf16[256,2048]{1,0:T(8,128)(2,1)} async-done(((bf16[128,2048]{1,0:T(8,128)(2,1)}), bf16[256,2048]{1,0:T(8,128)(2,1)}) %all-gather.18.cloned.1.call-update) | async-done | bytes 1048592 | tf_op jit(solution)/shard_map/all_gather | solution.py:63
  247.3 230.6 %all-gather.20.cloned.1.call-done = bf16[2048,4096]{1,0:T(8,128)(2,1)} async-done(((bf16[256,4096]{1,0:T(8,128)(2,1)}), bf16[2048,4096]{1,0:T(8,128)(2,1)}) %all-gather.20.cloned.1.call-update) | async-done | bytes 16777232 | tf_op jit(solution)/shard_map/all_gather | solution.py:64
  477.9 227.6 %all-gather.22.cloned.1.call-done = bf16[4096,2048]{1,0:T(8,128)(2,1)} async-done(((bf16[4096,256]{1,0:T(8,128)(2,1)}), bf16[4096,2048]{1,0:T(8,128)(2,1)}) %all-gather.22.cloned.1.call-update) | async-done | bytes 16777232 | tf_op jit(solution)/shard_map/all_gather | solution.py:67
  705.5 16.5 %convolution_convert_fusion = bf16[256,2048]{1,0:T(8,128)(2,1)} fusion(bf16[4096,2048]{1,0:T(8,128)(2,1)} %all-gather.22.cloned.1.call-done, bf16[256,2048]{1,0:T(8,128)(2,1)} %all-gather.18.cloned.1.call-done, bf16[2048,4096]{1,0:T(8,128)(2,1)} %all-gather.20.cloned.1.call-done), kind=kOutput, calls=%fused_computation.3 | convolution fusion | flops 8593604608 | bytes 35651584 | tf_op jit(solution)/shard_map/dot_general | solution.py:70
  722.1 6.7 reduce-scatter.5.cloned.1.call-done
  728.8 2.1 fusion.15
  (27 shorter events, 1.5 us)
Async XLA Ops:
  6.5 6.0 copy-start.3
  6.5 54.8 %all-gather.24.cloned.1.call-start = ((), (), s32[]{:S(2)}) async-start(), calls=%async_computation.11 | async-start | bytes 2359296 | tf_op jit(solution)/shard_map/all_gather | solution.py:10
  7.3 63.2 %all-gather.10.cloned.1.call-start = ((), (), s32[]{:S(2)}) async-start(), calls=%async_computation.2 | async-start | bytes 1572864 | tf_op jit(solution)/shard_map/all_gather | solution.py:32
  10.6 112.3 %all-gather.16.cloned.1.call-start = ((), (), s32[]{:S(2)}) async-start(), calls=%async_computation.5 | async-start | bytes 2359296 | tf_op jit(solution)/shard_map/all_gather | solution.py:35
  11.3 161.2 %all-gather.14.cloned.1.call-start = ((), (), s32[]{:S(2)}) async-start(), calls=%async_computation.4 | async-start | bytes 2359296 | tf_op jit(solution)/shard_map/all_gather | solution.py:37
  11.9 210.2 %all-gather.12.cloned.1.call-start = ((), (), s32[]{:S(2)}) async-start(), calls=%async_computation.3 | async-start | bytes 2359296 | tf_op jit(solution)/shard_map/all_gather | solution.py:36
  12.5 221.0 %reduce-scatter.3.cloned.1.call-start = ((), (), s32[]{:S(2)}) async-start(), calls=%async_computation.6 | async-start | bytes 1572864 | tf_op jit(solution)/shard_map/reduce_scatter | solution.py:55
  222.1 11.4 %copy-start = (bf16[128,2048]{1,0:T(8,128)(2,1)S(1)}, bf16[128,2048]{1,0:T(8,128)(2,1)}, u32[]{:S(2)}) copy-start(bf16[128,2048]{1,0:T(8,128)(2,1)} %param.10) | copy-start | bytes 1572868
  226.4 8.4 %copy-start.2 = (f32[2048]{0:T(1024)S(1)}, f32[2048]{0:T(1024)}, u32[]{:S(2)}) copy-start(f32[2048]{0:T(1024)} %param.17) | copy-start | bytes 24580
  226.5 20.9 %all-gather.18.cloned.1.call-start = ((), (), s32[]{:S(2)}) async-start(), calls=%async_computation.7 | async-start | bytes 1572864 | tf_op jit(solution)/shard_map/all_gather | solution.py:63
  236.9 241.0 %all-gather.20.cloned.1.call-start = ((), (), s32[]{:S(2)}) async-start(), calls=%async_computation.8 | async-start | bytes 18874368 | tf_op jit(solution)/shard_map/all_gather | solution.py:64
  237.7 467.8 %all-gather.22.cloned.1.call-start = ((), (), s32[]{:S(2)}) async-start(), calls=%async_computation.9 | async-start | bytes 18874368 | tf_op jit(solution)/shard_map/all_gather | solution.py:67
  238.4 490.4 %copy-start.1 = (bf16[128,2048]{1,0:T(8,128)(2,1)S(1)}, bf16[128,2048]{1,0:T(8,128)(2,1)}, u32[]{:S(2)}) copy-start(bf16[128,2048]{1,0:T(8,128)(2,1)} %reduce-scatter.3.cloned.1.call-done) | copy-start | bytes 1572868
  238.4 490.4 %reduce-scatter.5.cloned.1.call-start = ((), (), s32[]{:S(2)}) async-start(), calls=%async_computation.10 | async-start | bytes 1572864 | tf_op jit(solution)/shard_map/reduce_scatter | solution.py:69
Sparse Core Ops, SparseCore 0:
  9.5 51.7 all-gather.23
  62.8 7.5 all-gather.9
  72.6 50.2 all-gather.15
  124.8 47.6 all-gather.13
  174.5 47.6 all-gather.11
  226.6 6.8 reduce-scatter.2
  237.0 10.2 all-gather.17
  249.5 228.4 all-gather.19
  480.0 225.4 all-gather.21
  722.2 6.5 reduce-scatter.4
